TPU v7x, 32 devices: a whole 2x2x4 slice. The times are simulated.
32 devices in a mesh: grp: 2 (over y), fs: 4 (over z), tp: 4 (over x, core).
Axes of the slice: x: 2, y: 2, z: 4, core: 2. Of those that a mesh axis runs over, the one named last changes fastest.
Arguments:
- tokens: bfloat16 [2048, 4096], P(('grp', 'tp')), parts along dimension 0, may hold values from -6 to 6
- routes: int32 [2048, 2], P(('grp', 'tp')), parts along dimension 0, may hold values from 0 to 7, all different within a row; in each aligned block of 256 rows (0 to 255, 256 to 511, ...) at most 128 rows name the same one
- route_weight: float32 [2048, 2], P(('grp', 'tp')), parts along dimension 0, may hold values from 0.2 to 1
- norm_gain: float32 [4096], P('fs'), may hold values from 0.1 to 1.9
- gate_train: float32 [8, 4096, 2048], P(None, 'fs', 'tp'), may hold values from -0.09375 to 0.09375
- up_train: float32 [8, 4096, 2048], P(None, 'fs', 'tp'), may hold values from -0.09375 to 0.09375
- down_train: float32 [8, 2048, 4096], P(None, 'fs', 'tp'), may hold values from -0.125 to 0.125
Outputs:
- gate_serve: bfloat16 [16, 4096, 2048], P(('grp', 'tp'), None, 'fs'), parts along dimension 0
- up_serve: bfloat16 [16, 4096, 2048], P(('grp', 'tp'), None, 'fs'), parts along dimension 0
- down_serve: bfloat16 [16, 2048, 4096], P(('grp', 'tp'), 'fs'), parts along dimension 0
- moe_out: bfloat16 [2048, 4096], P(('grp', 'tp'), 'fs'), parts along dimension 0
There are 2 independent parts, one for each index of `grp`. A program takes and returns all parts, laid end to end along the dimension named above; an argument that names none is the same for every part. Nothing has to cross between parts.
Inputs may be any that keep to these rules, and one draw needn't show every extreme that they name: `routes`: within the 256 rows of each device (aligned blocks), no expert is named by more than 128 rows, a bound that some block reaches; the two experts of a row differ; every expert is named somewhere.
All inputs are finite; a program needn't handle non-finite values.
Results may differ from a plain program's by a relative error of at most 0.0076.
Values may be sent and summed in bfloat16 or wider, within the bound.
A program may use at most 192 MiB of HBM per device.

v0:
```python
import jax
import jax.numpy as jnp
from jax import lax
from jax.sharding import PartitionSpec as P

EXPERTS = 8
CAP = 128


def per_device(tokens, routes, route_weight, norm_gain, gate_train, up_train, down_train):
    gate_cast = (norm_gain[None, :, None] * gate_train).astype(jnp.bfloat16)
    up_cast = (norm_gain[None, :, None] * up_train).astype(jnp.bfloat16)
    down_cast = down_train.astype(jnp.bfloat16)
    gate_mid, up_mid, down_serve = (
        lax.all_to_all(gate_cast, "tp", split_axis=0, concat_axis=2, tiled=True),
        lax.all_to_all(up_cast, "tp", split_axis=0, concat_axis=2, tiled=True),
        lax.all_to_all(down_cast, "tp", split_axis=0, concat_axis=2, tiled=True),
    )
    gate_serve, up_serve = (
        lax.all_to_all(gate_mid, "fs", split_axis=2, concat_axis=1, tiled=True),
        lax.all_to_all(up_mid, "fs", split_axis=2, concat_axis=1, tiled=True),
    )
    tok_rows = tokens.shape[0]
    flat = routes.reshape(-1)
    expert_ids = jnp.arange(EXPERTS, dtype=jnp.int32)
    onehot = (flat[:, None] == expert_ids[None, :]).astype(jnp.int32)
    before = jnp.cumsum(onehot, axis=0) - onehot
    slot = jnp.sum(before * onehot, axis=1)
    place = (flat * CAP + slot).reshape(tok_rows, 2)
    slot_ids = jnp.arange(EXPERTS * CAP, dtype=jnp.int32)
    select = jnp.any(place[None, :, :] == slot_ids[:, None, None], axis=2).astype(jnp.bfloat16)
    outgoing = jnp.dot(select, tokens, preferred_element_type=jnp.float32).astype(jnp.bfloat16)
    arrived = lax.all_to_all(outgoing, "tp", split_axis=0, concat_axis=0, tiled=True)
    senders = lax.axis_size("tp")
    local = gate_serve.shape[0]
    arrived = arrived.reshape(senders, local, CAP, arrived.shape[1])
    gate_h = jnp.einsum("tlcd,ldf->tlcf", arrived, gate_serve, preferred_element_type=jnp.float32)
    up_h = jnp.einsum("tlcd,ldf->tlcf", arrived, up_serve, preferred_element_type=jnp.float32)
    hidden = (jax.nn.silu(gate_h) * up_h).astype(jnp.bfloat16)
    down_cols = lax.all_to_all(down_serve, "fs", split_axis=2, concat_axis=1, tiled=True)
    empty = jnp.zeros((down_cols.shape[2], senders * local * CAP), jnp.float32)
    term = jnp.einsum(
        "tlcf,lfd->dtlc",
        lax.all_gather(hidden, "fs", axis=3, tiled=True),
        down_cols,
        preferred_element_type=jnp.float32,
    )
    summed = term.reshape(empty.shape)
    returned = lax.all_to_all(
        summed.astype(jnp.bfloat16), "tp", split_axis=1, concat_axis=1, tiled=True
    )
    picked = jnp.take(returned, place, axis=1)
    mixed = (
        picked[:, :, 0].astype(jnp.float32) * route_weight[None, :, 0]
        + picked[:, :, 1].astype(jnp.float32) * route_weight[None, :, 1]
    )
    moe_out = mixed.T.astype(jnp.bfloat16)
    return (gate_serve, up_serve, down_serve, moe_out)


def solution(mesh):
    return jax.shard_map(
        per_device,
        mesh=mesh,
        in_specs=(
            P(("grp", "tp"), None),
            P(("grp", "tp"), None),
            P(("grp", "tp"), None),
            P("fs"),
            P(None, "fs", "tp"),
            P(None, "fs", "tp"),
            P(None, "fs", "tp"),
        ),
        out_specs=(
            P(("grp", "tp"), None, "fs"),
            P(("grp", "tp"), None, "fs"),
            P(("grp", "tp"), "fs", None),
            P(("grp", "tp"), "fs"),
        ),
        check_vma=False,
    )
```

profile of v0, /device:TPU:0, one launch (start us, length us, event | category | flops | bytes accessed | tf_op | source)
XLA Modules:
  0.0 1133.6 jit_solution(945579070629410904)
XLA Ops:
  7.2 0.0 copy-start
  7.2 1.0 copy.104
  8.1 0.1 eq.42
  8.3 0.1 eq.38
  8.4 1.1 reduce-window.6
  9.6 0.2 slice_reduce_fusion
  9.9 0.1 fusion.19
  9.9 0.1 reduce_sum.12
  10.1 0.1 copy.106
  10.2 1.3 compare_and_fusion
  11.4 0.4 fusion.9
  11.8 0.0 copy-done
  11.8 5.7 convolution_convert_fusion
  17.6 5.8 all-to-all-start.5
  23.3 0.0 copy-done.3
  23.4 17.0 %multiply_convert_fusion = (bf16[8,1024,512]{2,1,0:T(8,128)(2,1)}, bf16[8,1024,512]{2,1,0:T(8,128)(2,1)}) fusion(f32[8,1024,512]{2,1,0:T(8,128)} %param.12, f32[1024]{0:T(1024)S(1)} %copy-done.3, f32[8,1024,512]{2,1,0:T(8,128)} %param.11), kind=kLoop, calls=%fused_computation.1 | loop fusion | flops 16777216 | bytes 50335744 | tf_op jit(solution)/shard_map/convert_element_type | solution.py:12
  40.4 76.8 %all-to-all-done.5 = bf16[4,256,4096]{2,1,0:T(8,128)(2,1)} async-done(((bf16[4,256,4096]{2,1,0:T(8,128)(2,1)}), bf16[4,256,4096]{2,1,0:T(8,128)(2,1)}, u32[]{:S(2)}, u32[]{:S(2)}) %all-to-all-start.5) | async-done | bytes 8388640 | tf_op jit(solution)/shard_map/all_to_all | solution.py:33
  117.2 100.5 %all_to_all.126 = bf16[8,1024,512]{2,1,0:T(8,128)(2,1)} all-to-all(bf16[8,1024,512]{2,1,0:T(8,128)(2,1)} %get-tuple-element.30), channel_id=1, replica_groups=mesh['grp'=2,'fs'=4,'tp'=4] {'tp'}, dimensions={0} | all-to-all | bytes 16777216 | tf_op jit(solution)/shard_map/all_to_all | solution.py:16
  217.7 5.7 all-to-all-start
  223.4 9.1 convert_element_type.53
  232.5 84.1 %all-to-all-done = bf16[8,1024,512]{2,1,0:T(8,128)(2,1)} async-done(((bf16[8,1024,512]{2,1,0:T(8,128)(2,1)}), bf16[8,1024,512]{2,1,0:T(8,128)(2,1)}, u32[]{:S(2)}, u32[]{:S(2)}) %all-to-all-start) | async-done | bytes 8388640 | tf_op jit(solution)/shard_map/all_to_all | solution.py:15
  316.5 5.6 all-to-all-start.4
  322.1 11.4 %copy.99 = bf16[2,1024,4,512]{1,3,2,0:T(8,128)(2,1)} copy(bf16[2,1024,4,512]{3,1,0,2:T(8,128)(2,1)} %bitcast.96) | data formatting | bytes 16777216 | tf_op jit(solution)/shard_map/all_to_all | solution.py:16
  333.5 16.4 %copy.100 = bf16[2,1024,2048]{1,0,2:T(2,128)(2,1)} copy(bf16[2,1024,2048]{1,2,0:T(8,128)(2,1)} %bitcast.97) | data formatting | bytes 16777216 | tf_op jit(solution)/shard_map/all_to_all | solution.py:16
  349.9 65.4 %all-to-all-done.4 = bf16[8,512,1024]{2,1,0:T(8,128)(2,1)} async-done(((bf16[8,512,1024]{2,1,0:T(8,128)(2,1)}), bf16[8,512,1024]{2,1,0:T(8,128)(2,1)}, u32[]{:S(2)}, u32[]{:S(2)}) %all-to-all-start.4) | async-done | bytes 8388640 | tf_op jit(solution)/shard_map/all_to_all | solution.py:17
  415.3 5.7 all-to-all-start.3
  421.0 11.4 %copy.95 = bf16[2,1024,4,512]{1,3,2,0:T(8,128)(2,1)} copy(bf16[2,1024,4,512]{3,1,0,2:T(8,128)(2,1)} %bitcast.1) | data formatting | bytes 16777216 | tf_op jit(solution)/shard_map/all_to_all | solution.py:15
  432.3 16.4 %copy.96 = bf16[2,1024,2048]{1,0,2:T(2,128)(2,1)} copy(bf16[2,1024,2048]{1,2,0:T(8,128)(2,1)} %bitcast.98) | data formatting | bytes 16777216 | tf_op jit(solution)/shard_map/all_to_all | solution.py:15
  448.7 156.0 %all-to-all-done.3 = bf16[2,1024,2048]{1,0,2:T(2,128)(2,1)} async-done(((bf16[2,1024,2048]{1,0,2:T(2,128)(2,1)}), bf16[2,1024,2048]{1,0,2:T(2,128)(2,1)}, u32[]{:S(2)}, u32[]{:S(2)}) %all-to-all-start.3) | async-done | bytes 8388640 | tf_op jit(solution)/shard_map/all_to_all | solution.py:21
  604.7 5.7 all-to-all-start.1
  610.4 21.1 %copy.103 = bf16[4,2,512,1024]{2,1,3,0:T(2,128)(2,1)} copy(bf16[4,2,512,1024]{3,2,1,0:T(8,128)(2,1)} %bitcast.11) | data formatting | bytes 16777216 | tf_op jit(solution)/shard_map/all_to_all | solution.py:17
  631.5 161.5 %all-to-all-done.1 = bf16[2,1024,2048]{1,0,2:T(2,128)(2,1)} async-done(((bf16[2,1024,2048]{1,0,2:T(2,128)(2,1)}), bf16[2,1024,2048]{1,0,2:T(2,128)(2,1)}, u32[]{:S(2)}, u32[]{:S(2)}) %all-to-all-start.1) | async-done | bytes 8388640 | tf_op jit(solution)/shard_map/all_to_all | solution.py:20
  792.9 5.6 all-to-all-start.6
  798.6 0.2 all-gather.2.cloned.1.call-start
  798.8 9.4 copy.101
  808.2 11.4 %copy.102 = bf16[2,4,1024,512]{3,2,1,0:T(8,128)(2,1)} copy(bf16[2,4,1024,512]{2,3,1,0:T(8,128)(2,1)} %bitcast.99) | data formatting | bytes 16777216 | tf_op jit(solution)/shard_map/all_to_all | solution.py:21
  819.6 9.3 copy.97
  828.9 12.2 %copy.98 = bf16[2,4,1024,512]{2,1,3,0:T(4,128)(2,1)} copy(bf16[2,4,1024,512]{2,3,1,0:T(8,128)(2,1)} %bitcast.93) | data formatting | bytes 16777216 | tf_op jit(solution)/shard_map/all_to_all | solution.py:20
  841.1 14.4 %reshape.71 = bf16[2,4096,512,1]{1,2,0,3:T(8,128)(2,1)} reshape(bf16[2,4,1024,512]{2,1,3,0:T(4,128)(2,1)} %copy.98) | data formatting | bytes 16777216 | tf_op jit(solution)/shard_map/all_to_all | solution.py:20
  855.5 10.3 fusion.2
  865.8 0.0 copy-done.2
  865.8 8.5 fusion.5
  874.4 0.0 all-gather.2.cloned.1.call-update
  874.4 174.2 %all-to-all-done.6 = bf16[2,512,4096]{1,0,2:T(2,128)(2,1)} async-done(((bf16[2,512,4096]{1,0,2:T(2,128)(2,1)}), bf16[2,512,4096]{1,0,2:T(2,128)(2,1)}, u32[]{:S(2)}, u32[]{:S(2)}) %all-to-all-start.6) | async-done | bytes 8388640 | tf_op jit(solution)/shard_map/all_to_all | solution.py:40
  1048.6 21.0 %copy.110 = bf16[2,512,4,1024]{3,1,2,0:T(8,128)(2,1)} copy(bf16[2,512,4,1024]{1,0,3,2:T(2,128)(2,1)} %bitcast.23) | data formatting | bytes 16777216 | tf_op jit(solution)/shard_map/all_to_all | solution.py:40
  1069.6 9.2 convert_bitcast_fusion
  1078.8 0.0 copy-start.7
  1078.8 1.5 copy.112
  1080.3 4.4 all-to-all-start.7
  1084.8 0.1 copy.113
  1084.9 0.1 reshape.63
  1085.1 0.0 copy-done.7
  1085.1 0.6 fusion.21
  1085.7 21.0 %copy.116 = bf16[2,512,4096]{2,1,0:T(8,128)(2,1)} copy(bf16[2,512,4096]{1,0,2:T(2,128)(2,1)} %bitcast.92) | data formatting | bytes 16777216
  1106.7 11.4 %copy.123 = bf16[2,4,1024,512]{3,2,1,0:T(8,128)(2,1)} copy(bf16[2,4,1024,512]{2,3,1,0:T(8,128)(2,1)} %bitcast.94) | data formatting | bytes 16777216
  1118.1 0.0 all-to-all-done.7
  1118.1 0.0 copy-start.6
  1118.1 0.0 copy-start.1
  1118.1 4.7 gather_fusion
  1122.8 1.2 reshape.66
  1124.1 0.0 copy-done.4
  1124.1 1.6 fusion.16
  1125.7 0.0 copy-done.5
  1125.7 1.0 fusion.17
  (12 shorter events, 0.1 us)
Async XLA Ops:
  7.2 4.7 copy-start
  17.6 5.8 copy-start.3
  17.6 99.6 %all-to-all-start.5 = ((bf16[4,256,4096]{2,1,0:T(8,128)(2,1)}), bf16[4,256,4096]{2,1,0:T(8,128)(2,1)}, u32[]{:S(2)}, u32[]{:S(2)}) async-start(bf16[4,256,4096]{2,1,0:T(8,128)(2,1)} %bitcast.95), calls=%async_computation.5 | async-start | bytes 16777216 | tf_op jit(solution)/shard_map/all_to_all | solution.py:33
  217.7 98.8 %all-to-all-start = ((bf16[8,1024,512]{2,1,0:T(8,128)(2,1)}), bf16[8,1024,512]{2,1,0:T(8,128)(2,1)}, u32[]{:S(2)}, u32[]{:S(2)}) async-start(bf16[8,1024,512]{2,1,0:T(8,128)(2,1)} %get-tuple-element.31), calls=%async_computation | async-start | bytes 16777216 | tf_op jit(solution)/shard_map/all_to_all | solution.py:15
  316.5 98.8 %all-to-all-start.4 = ((bf16[8,512,1024]{2,1,0:T(8,128)(2,1)}), bf16[8,512,1024]{2,1,0:T(8,128)(2,1)}, u32[]{:S(2)}, u32[]{:S(2)}) async-start(bf16[8,512,1024]{2,1,0:T(8,128)(2,1)} %convert_element_type.53), calls=%async_computation.4 | async-start | bytes 16777216 | tf_op jit(solution)/shard_map/all_to_all | solution.py:17
  415.3 189.4 %all-to-all-start.3 = ((bf16[2,1024,2048]{1,0,2:T(2,128)(2,1)}), bf16[2,1024,2048]{1,0,2:T(2,128)(2,1)}, u32[]{:S(2)}, u32[]{:S(2)}) async-start(bf16[2,1024,2048]{1,0,2:T(2,128)(2,1)} %copy.100), calls=%async_computation.3 | async-start | bytes 16777216 | tf_op jit(solution)/shard_map/all_to_all | solution.py:21
  604.7 188.2 %all-to-all-start.1 = ((bf16[2,1024,2048]{1,0,2:T(2,128)(2,1)}), bf16[2,1024,2048]{1,0,2:T(2,128)(2,1)}, u32[]{:S(2)}, u32[]{:S(2)}) async-start(bf16[2,1024,2048]{1,0,2:T(2,128)(2,1)} %copy.96), calls=%async_computation.1 | async-start | bytes 16777216 | tf_op jit(solution)/shard_map/all_to_all | solution.py:20
  792.9 255.7 %all-to-all-start.6 = ((bf16[2,512,4096]{1,0,2:T(2,128)(2,1)}), bf16[2,512,4096]{1,0,2:T(2,128)(2,1)}, u32[]{:S(2)}, u32[]{:S(2)}) async-start(bf16[2,512,4096]{1,0,2:T(2,128)(2,1)} %bitcast.91), calls=%async_computation.6 | async-start | bytes 16777216 | tf_op jit(solution)/shard_map/all_to_all | solution.py:40
  798.6 271.1 %all-gather.2.cloned.1.call-start = ((), (), s32[]{:S(2)}) async-start(), calls=%async_computation.8 | async-start | bytes 5242880 | tf_op jit(solution)/shard_map/all_gather | solution.py:44
  855.5 10.4 copy-start.2
  1078.8 6.3 copy-start.7
  1080.3 37.8 %all-to-all-start.7 = ((bf16[1024,4,256]{0,2,1:T(8,128)(2,1)}), bf16[1024,4,256]{0,2,1:T(8,128)(2,1)}, u32[]{:S(2)}, u32[]{:S(2)}) async-start(bf16[1024,4,256]{0,2,1:T(8,128)(2,1)} %bitcast.29), calls=%async_computation.7 | async-start | bytes 4194304 | tf_op jit(solution)/shard_map/all_to_all | solution.py:49
  1118.1 6.0 copy-start.4
  1118.1 7.6 copy-start.5
  1118.1 7.6 copy-start.6
  1118.1 8.7 copy-start.1
Sparse Core Ops, SparseCore 0:
  874.5 159.5 all-gather.1
where the time goes:
time: 1140 us; the launch traced here: 1130 us
  waiting for transfers between devices  718 us (63%)
  local copies, waits for them, and re-layouts  197 us (17%)
  blocking collectives  101 us (9%)
  starting transfers between devices  38.7 us (3%)
  matrix products  33.8 us (3%)
  other arithmetic  31.7 us (3%)
  between operations  14.3 us (1%)
    all_to_all x1, waiting for transfers between devices, per_device(): lax.all_to_all(down_serve, 'fs', split_axis=2, concat_axis=1, tiled=True)  174 us
    all_to_all x1, waiting for transfers between devices, per_device(): lax.all_to_all(gate_mid, 'fs', split_axis=2, concat_axis=1, tiled=True)  161 us
    all_to_all x1, waiting for transfers between devices, per_device(): lax.all_to_all(up_mid, 'fs', split_axis=2, concat_axis=1, tiled=True)  156 us
    all_to_all x1, blocking collectives, per_device(): lax.all_to_all(up_cast, 'tp', split_axis=0, concat_axis=2, tiled=True)  101 us
    all_to_all x1, waiting for transfers between devices, per_device(): lax.all_to_all(gate_cast, 'tp', split_axis=0, concat_axis=2, tiled=True)  84.1 us
    all_to_all x1, waiting for transfers between devices, per_device(): lax.all_to_all(outgoing, 'tp', split_axis=0, concat_axis=0, tiled=True)  76.8 us
    all_to_all x1, waiting for transfers between devices, per_device(): lax.all_to_all(down_cast, 'tp', split_axis=0, concat_axis=2, tiled=True)  65.4 us
    all_to_all x3, local copies, waits for them, and re-layouts, per_device(): lax.all_to_all(gate_mid, 'fs', split_axis=2, concat_axis=1, tiled=True)  35.8 us
  transfers between devices with their start and end apart: 8, of which 6 were waited for; matrix products, arithmetic and copies ran while one was open for 21% of the time, Pallas kernels for 0%

commit v1 on v0

--- a/solution.py
+++ b/solution.py
@@ -12,7 +12,12 @@
     up_cast = (norm_gain[None, :, None] * up_train).astype(jnp.bfloat16)
     down_cast = down_train.astype(jnp.bfloat16)
     gate_mid, up_mid, down_serve = (
-        lax.all_to_all(gate_cast, "tp", split_axis=0, concat_axis=2, tiled=True),
+        jnp.concatenate(
+            lax.all_to_all(
+                jnp.stack(jnp.split(gate_cast, lax.axis_size("tp"), axis=0)), "tp", 0, 0
+            ),
+            axis=2,
+        ),
         lax.all_to_all(up_cast, "tp", split_axis=0, concat_axis=2, tiled=True),
         lax.all_to_all(down_cast, "tp", split_axis=0, concat_axis=2, tiled=True),
     )

time: 1140 us -> 1160 us (1.018)
    all_to_all x2 -> x1, local copies, waits for them, and re-layouts: 27.7 us -> 7.76 us  [per_device(): lax.all_to_all(jnp.stack(jnp.split(gate_cast, lax.axis_size('tp'), axis=0...]
    reshape x0 -> x1, local copies, waits for them, and re-layouts: none -> 16.4 us  [per_device(): jnp.concatenate(lax.all_to_all(jnp.stack(jnp.split(gate_cast, lax.axis_si...]
    another operation x1 -> x3, local copies, waits for them, and re-layouts: 0.01 us -> 12.1 us  [the longest x2 12 us: per_device(): jnp.stack(jnp.split(gate_cast, lax.axis_size('tp'), axis=0))]
    unnamed x19 -> x17, local copies, waits for them, and re-layouts: 33.4 us -> 32.6 us
  transfers between devices with their start and end apart: 8 -> 8, of which waited for: 6 -> 6; matrix products, arithmetic and copies ran while one was open for 21% -> 19% of each run, Pallas kernels for 0% -> 0%
where the time goes in v1:
time: 1160 us; the launch traced here: 1150 us
  waiting for transfers between devices  728 us (63%)
  local copies, waits for them, and re-layouts  204 us (18%)
  blocking collectives  101 us (9%)
  starting transfers between devices  38.7 us (3%)
  matrix products  35.7 us (3%)
  other arithmetic  33 us (3%)
  between operations  14.3 us (1%)
    all_to_all x1, waiting for transfers between devices, per_device(): lax.all_to_all(down_serve, 'fs', split_axis=2, concat_axis=1, tiled=True)  172 us
    all_to_all x1, waiting for transfers between devices, per_device(): lax.all_to_all(up_mid, 'fs', split_axis=2, concat_axis=1, tiled=True)  162 us
    all_to_all x1, waiting for transfers between devices, per_device(): lax.all_to_all(gate_mid, 'fs', split_axis=2, concat_axis=1, tiled=True)  156 us
    all_to_all x1, blocking collectives, per_device(): lax.all_to_all(outgoing, 'tp', split_axis=0, concat_axis=0, tiled=True)  101 us
    all_to_all x1, waiting for transfers between devices, per_device(): lax.all_to_all(jnp.stack(jnp.split(gate_cast, lax.axis_size('tp'), axis=0...  84.9 us
    all_to_all x1, waiting for transfers between devices, per_device(): lax.all_to_all(up_cast, 'tp', split_axis=0, concat_axis=2, tiled=True)  84.1 us
    all_to_all x1, waiting for transfers between devices, per_device(): lax.all_to_all(down_cast, 'tp', split_axis=0, concat_axis=2, tiled=True)  69 us
    all_to_all x3, local copies, waits for them, and re-layouts, per_device(): lax.all_to_all(gate_mid, 'fs', split_axis=2, concat_axis=1, tiled=True)  35.8 us
  transfers between devices with their start and end apart: 8, of which 6 were waited for; matrix products, arithmetic and copies ran while one was open for 19% of the time, Pallas kernels for 0%

profile of v1, /device:TPU:0, one launch (start us, length us, event | category | flops | bytes accessed | tf_op | source)
XLA Modules:
  0.0 1154.4 jit_solution(17331748421417549773)
XLA Ops:
  7.2 0.0 copy-start
  7.2 15.1 %multiply_convert_fusion = (bf16[8,1024,512]{2,1,0:T(8,128)(2,1)}, bf16[8,1024,512]{2,1,0:T(8,128)(2,1)S(1)}) fusion(f32[8,1024,512]{2,1,0:T(8,128)} %param.12, f32[1024]{0:T(1024)} %param.10, f32[8,1024,512]{2,1,0:T(8,128)} %param.11), kind=kLoop, calls=%fused_computation.1 | loop fusion | flops 16777216 | bytes 50335744 | tf_op jit(solution)/shard_map/convert_element_type | solution.py:12
  22.3 0.7 slice_bitcast_fusion.3
  23.0 3.9 pad_maximum_fusion
  26.8 11.4 copy.131
  38.2 5.8 all-to-all-start
  44.0 0.0 copy-done.2
  44.0 0.1 copy.141
  44.1 0.1 eq.42
  44.3 0.1 eq.38
  44.4 1.1 reduce-window.6
  45.6 0.2 slice_reduce_fusion
  45.8 0.1 fusion.19
  45.9 0.1 reduce_sum.12
  46.1 0.1 copy.143
  46.1 0.6 compare_and_fusion
  46.7 0.4 fusion.9
  47.1 0.0 copy-done
  47.1 5.7 convolution_convert_fusion
  52.9 84.9 %all-to-all-done = bf16[4,2,1024,512]{2,3,1,0:T(8,128)(2,1)} async-done(((bf16[4,2,1024,512]{2,3,1,0:T(8,128)(2,1)}), bf16[4,2,1024,512]{2,3,1,0:T(8,128)(2,1)}, u32[]{:S(2)}, u32[]{:S(2)}) %all-to-all-start) | async-done | bytes 8388640 | tf_op jit(solution)/shard_map/all_to_all | solution.py:16
  137.8 100.6 %all_to_all.113 = bf16[4,256,4096]{2,1,0:T(8,128)(2,1)} all-to-all(bf16[4,256,4096]{2,1,0:T(8,128)(2,1)} %bitcast.102), channel_id=1, replica_groups=mesh['grp'=2,'fs'=4,'tp'=4] {'tp'}, dimensions={0} | all-to-all | bytes 16777216 | tf_op jit(solution)/shard_map/all_to_all | solution.py:38
  238.4 5.6 all-to-all-start.2
  244.0 9.1 convert_element_type.53
  253.1 84.1 %all-to-all-done.2 = bf16[8,1024,512]{2,1,0:T(8,128)(2,1)} async-done(((bf16[8,1024,512]{2,1,0:T(8,128)(2,1)}), bf16[8,1024,512]{2,1,0:T(8,128)(2,1)}, u32[]{:S(2)}, u32[]{:S(2)}) %all-to-all-start.2) | async-done | bytes 8388640 | tf_op jit(solution)/shard_map/all_to_all | solution.py:21
  337.2 5.7 all-to-all-start.4
  342.8 7.8 copy.132
  350.6 16.4 %copy.133 = bf16[2,1024,2048]{1,0,2:T(2,128)(2,1)} copy(bf16[2,1024,2048]{1,2,0:T(8,128)(2,1)} %bitcast.103) | data formatting | bytes 16777216 | tf_op jit(solution)/shard_map/reshape | solution.py:15
  367.0 69.0 %all-to-all-done.4 = bf16[8,512,1024]{2,1,0:T(8,128)(2,1)} async-done(((bf16[8,512,1024]{2,1,0:T(8,128)(2,1)}), bf16[8,512,1024]{2,1,0:T(8,128)(2,1)}, u32[]{:S(2)}, u32[]{:S(2)}) %all-to-all-start.4) | async-done | bytes 8388640 | tf_op jit(solution)/shard_map/all_to_all | solution.py:22
  436.0 5.7 all-to-all-start.1
  441.6 11.4 copy.136
  453.0 16.4 %copy.137 = bf16[2,1024,2048]{1,0,2:T(2,128)(2,1)} copy(bf16[2,1024,2048]{1,2,0:T(8,128)(2,1)} %bitcast.104) | data formatting | bytes 16777216 | tf_op jit(solution)/shard_map/all_to_all | solution.py:21
  469.4 156.0 %all-to-all-done.1 = bf16[2,1024,2048]{1,0,2:T(2,128)(2,1)} async-done(((bf16[2,1024,2048]{1,0,2:T(2,128)(2,1)}), bf16[2,1024,2048]{1,0,2:T(2,128)(2,1)}, u32[]{:S(2)}, u32[]{:S(2)}) %all-to-all-start.1) | async-done | bytes 8388640 | tf_op jit(solution)/shard_map/all_to_all | solution.py:25
  625.4 5.7 all-to-all-start.3
  631.1 21.1 %copy.140 = bf16[4,2,512,1024]{2,1,3,0:T(2,128)(2,1)} copy(bf16[4,2,512,1024]{3,2,1,0:T(8,128)(2,1)} %bitcast.14) | data formatting | bytes 16777216 | tf_op jit(solution)/shard_map/all_to_all | solution.py:22
  652.2 161.5 %all-to-all-done.3 = bf16[2,1024,2048]{1,0,2:T(2,128)(2,1)} async-done(((bf16[2,1024,2048]{1,0,2:T(2,128)(2,1)}), bf16[2,1024,2048]{1,0,2:T(2,128)(2,1)}, u32[]{:S(2)}, u32[]{:S(2)}) %all-to-all-start.3) | async-done | bytes 8388640 | tf_op jit(solution)/shard_map/all_to_all | solution.py:26
  813.7 5.6 all-to-all-start.6
  819.3 0.2 all-gather.2.cloned.1.call-start
  819.6 9.3 copy.134
  828.8 12.2 %copy.135 = bf16[2,4,1024,512]{2,1,3,0:T(4,128)(2,1)} copy(bf16[2,4,1024,512]{2,3,1,0:T(8,128)(2,1)} %bitcast.100) | data formatting | bytes 16777216 | tf_op jit(solution)/shard_map/all_to_all | solution.py:25
  841.0 14.3 %reshape.79 = bf16[2,4096,512,1]{1,2,0,3:T(8,128)(2,1)} reshape(bf16[2,4,1024,512]{2,1,3,0:T(4,128)(2,1)} %copy.135) | data formatting | bytes 16777216 | tf_op jit(solution)/shard_map/all_to_all | solution.py:25
  855.3 9.4 copy.138
  864.8 11.4 copy.139
  876.2 10.2 fusion.2
  886.4 10.6 fusion.5
  897.0 0.0 all-gather.2.cloned.1.call-update
  897.0 172.4 %all-to-all-done.6 = bf16[2,512,4096]{1,0,2:T(2,128)(2,1)} async-done(((bf16[2,512,4096]{1,0,2:T(2,128)(2,1)}), bf16[2,512,4096]{1,0,2:T(2,128)(2,1)}, u32[]{:S(2)}, u32[]{:S(2)}) %all-to-all-start.6) | async-done | bytes 8388640 | tf_op jit(solution)/shard_map/all_to_all | solution.py:45
  1069.4 21.0 %copy.147 = bf16[2,512,4,1024]{3,1,2,0:T(8,128)(2,1)} copy(bf16[2,512,4,1024]{1,0,3,2:T(2,128)(2,1)} %bitcast.26) | data formatting | bytes 16777216 | tf_op jit(solution)/shard_map/all_to_all | solution.py:45
  1090.4 9.2 convert_bitcast_fusion
  1099.6 0.0 copy-start.6
  1099.7 1.5 copy.149
  1101.1 4.5 all-to-all-start.7
  1105.6 0.1 copy.150
  1105.7 0.1 reshape.71
  1105.9 0.0 copy-done.6
  1105.9 0.6 fusion.21
  1106.5 21.0 %copy.153 = bf16[2,512,4096]{2,1,0:T(8,128)(2,1)} copy(bf16[2,512,4096]{1,0,2:T(2,128)(2,1)} %bitcast.99) | data formatting | bytes 16777216
  1127.5 11.4 copy.160
  1138.9 0.0 all-to-all-done.7
  1138.9 0.0 copy-start.5
  1138.9 0.0 copy-start.1
  1138.9 4.7 gather_fusion
  1143.7 1.2 reshape.74
  1144.9 1.6 fusion.16
  1146.5 1.0 fusion.17
  (13 shorter events, 0.1 us)
Async XLA Ops:
  7.2 39.9 %copy-start = (bf16[256,4096]{1,0:T(8,128)(2,1)S(1)}, bf16[256,4096]{1,0:T(8,128)(2,1)}, u32[]{:S(2)}) copy-start(bf16[256,4096]{1,0:T(8,128)(2,1)} %param.7) | copy-start | bytes 6291460
  38.2 5.8 copy-start.2
  38.2 99.6 %all-to-all-start = ((bf16[4,2,1024,512]{2,3,1,0:T(8,128)(2,1)}), bf16[4,2,1024,512]{2,3,1,0:T(8,128)(2,1)}, u32[]{:S(2)}, u32[]{:S(2)}) async-start(bf16[4,2,1024,512]{2,3,1,0:T(8,128)(2,1)} %copy.131), calls=%async_computation | async-start | bytes 16777216 | tf_op jit(solution)/shard_map/all_to_all | solution.py:16
  238.4 98.8 %all-to-all-start.2 = ((bf16[8,1024,512]{2,1,0:T(8,128)(2,1)}), bf16[8,1024,512]{2,1,0:T(8,128)(2,1)}, u32[]{:S(2)}, u32[]{:S(2)}) async-start(bf16[8,1024,512]{2,1,0:T(8,128)(2,1)} %get-tuple-element.38), calls=%async_computation.2 | async-start | bytes 16777216 | tf_op jit(solution)/shard_map/all_to_all | solution.py:21
  337.2 98.8 %all-to-all-start.4 = ((bf16[8,512,1024]{2,1,0:T(8,128)(2,1)}), bf16[8,512,1024]{2,1,0:T(8,128)(2,1)}, u32[]{:S(2)}, u32[]{:S(2)}) async-start(bf16[8,512,1024]{2,1,0:T(8,128)(2,1)} %convert_element_type.53), calls=%async_computation.4 | async-start | bytes 16777216 | tf_op jit(solution)/shard_map/all_to_all | solution.py:22
  436.0 189.5 %all-to-all-start.1 = ((bf16[2,1024,2048]{1,0,2:T(2,128)(2,1)}), bf16[2,1024,2048]{1,0,2:T(2,128)(2,1)}, u32[]{:S(2)}, u32[]{:S(2)}) async-start(bf16[2,1024,2048]{1,0,2:T(2,128)(2,1)} %copy.133), calls=%async_computation.1 | async-start | bytes 16777216 | tf_op jit(solution)/shard_map/all_to_all | solution.py:25
  625.4 188.3 %all-to-all-start.3 = ((bf16[2,1024,2048]{1,0,2:T(2,128)(2,1)}), bf16[2,1024,2048]{1,0,2:T(2,128)(2,1)}, u32[]{:S(2)}, u32[]{:S(2)}) async-start(bf16[2,1024,2048]{1,0,2:T(2,128)(2,1)} %copy.137), calls=%async_computation.3 | async-start | bytes 16777216 | tf_op jit(solution)/shard_map/all_to_all | solution.py:26
  813.7 255.7 %all-to-all-start.6 = ((bf16[2,512,4096]{1,0,2:T(2,128)(2,1)}), bf16[2,512,4096]{1,0,2:T(2,128)(2,1)}, u32[]{:S(2)}, u32[]{:S(2)}) async-start(bf16[2,512,4096]{1,0,2:T(2,128)(2,1)} %bitcast.98), calls=%async_computation.6 | async-start | bytes 16777216 | tf_op jit(solution)/shard_map/all_to_all | solution.py:45
  819.3 271.1 %all-gather.2.cloned.1.call-start = ((), (), s32[]{:S(2)}) async-start(), calls=%async_computation.8 | async-start | bytes 5242880 | tf_op jit(solution)/shard_map/all_gather | solution.py:49
  1099.6 6.3 copy-start.6
  1101.1 37.8 %all-to-all-start.7 = ((bf16[1024,4,256]{0,2,1:T(8,128)(2,1)}), bf16[1024,4,256]{0,2,1:T(8,128)(2,1)}, u32[]{:S(2)}, u32[]{:S(2)}) async-start(bf16[1024,4,256]{0,2,1:T(8,128)(2,1)} %bitcast.32), calls=%async_computation.7 | async-start | bytes 4194304 | tf_op jit(solution)/shard_map/all_to_all | solution.py:54
  1138.9 6.0 copy-start.3
  1138.9 7.6 copy-start.4
  1138.9 7.6 copy-start.5
  1138.9 8.7 copy-start.1
Sparse Core Ops, SparseCore 0:
  897.1 159.5 all-gather.1
